TPU v7x, 32 devices: a whole 2x2x4 slice. The times are simulated.
32 devices in a mesh: ep: 16 (over z, y, x), tp: 2 (over core).
Axes of the slice: x: 2, y: 2, z: 4, core: 2. Of those that a mesh axis runs over, the one named last changes fastest.
Arguments:
- hidden: bfloat16 [256, 2048], P('ep'), may hold values from -6 to 6
- attn_gain: bfloat16 [2048], replicated, may hold values from 0.099609375 to 1.8984375
- query_weight: bfloat16 [2048, 2048], P(None, 'tp'), may hold values from -0.125 to 0.125
- key_weight: bfloat16 [2048, 128], P(None, 'tp'), may hold values from -0.125 to 0.125
- value_weight: bfloat16 [2048, 128], P(None, 'tp'), may hold values from -0.125 to 0.125
- forget_weight: bfloat16 [2048, 32], P(None, 'tp'), may hold values from -0.125 to 0.125
- forget_bias: float32 [32], P('tp'), may hold values from -1 to 4
- cache_keys: bfloat16 [256, 2, 64, 1024], P('ep', 'tp'), may hold values from -64 to 64
- cache_values: bfloat16 [256, 2, 64, 1024], P('ep', 'tp'), may hold values from -6 to 6
- cache_logsum: float32 [256, 32, 1024], P('ep', 'tp'), may hold values from -144 to 0, as said below
- lengths: int32 [256], P('ep'), may hold values from 2 to 1023, as said below
- out_weight: bfloat16 [2048, 2048], P('ep'), may hold values from -0.125 to 0.125
- ffn_gain: bfloat16 [2048], replicated, may hold values from 0.099609375 to 1.8984375
- expert_ids: int32 [256, 6], P('ep'), may hold values from 0 to 15, all different within a row; in each aligned block of 16 rows (0 to 15, 16 to 31, ...) at most 12 rows name the same one
- expert_scores: float32 [256, 6], P('ep'), may hold values from 0.1 to 1
- gate_weights: bfloat16 [16, 2048, 512], P('ep', None, 'tp'), may hold values from -0.125 to 0.125
- up_weights: bfloat16 [16, 2048, 512], P('ep', None, 'tp'), may hold values from -0.125 to 0.125
- down_weights: bfloat16 [16, 512, 2048], P('ep', 'tp'), may hold values from -0.25 to 0.25
Outputs:
- updated: bfloat16 [256, 2048], P('ep')
- new_key: bfloat16 [256, 2, 64], P('ep', 'tp')
- new_value: bfloat16 [256, 2, 64], P('ep', 'tp')
- new_logsum: float32 [256, 32], P('ep', 'tp')
Inputs may be any that keep to these rules, and one draw needn't show every extreme that they name: `cache_logsum`: non-increasing along the positions. The new token stands at position lengths; some sequence has 1023 cached positions. `expert_ids`: each row names 6 different experts; the rows of one index of ep name one expert at most 12 times.
All inputs are finite; a program needn't handle non-finite values.
Results may differ from a plain program's by a relative error of at most 0.006.
Values may be sent and summed in bfloat16 or wider, within the bound.
A program may use at most 64 MiB of HBM per device.

v0:
```python
import jax
import jax.numpy as jnp
from jax import lax
from jax.sharding import PartitionSpec as P

HD = 64
TOP_K = 6
epsilon = 1e-06


def root_norm(values_in, gain):
    floats = values_in.astype(jnp.float32)
    inv_root = lax.rsqrt(jnp.mean(floats * floats, axis=-1, keepdims=True) + epsilon)
    return floats * inv_root * gain.astype(jnp.float32)


def per_device(
    hidden,
    attn_gain,
    query_weight,
    key_weight,
    value_weight,
    forget_weight,
    forget_bias,
    cache_keys,
    cache_values,
    cache_logsum,
    lengths,
    out_weight,
    ffn_gain,
    expert_ids,
    expert_scores,
    gate_weights,
    up_weights,
    down_weights,
):
    rows_here = hidden.shape[0]
    query_heads = query_weight.shape[1] // HD
    key_heads = key_weight.shape[1] // HD
    group_size = query_heads // key_heads
    cache_len = cache_keys.shape[-1]
    score_scale = HD ** (-0.5)
    normed = root_norm(hidden, attn_gain).astype(jnp.bfloat16)
    queries = jnp.dot(normed, query_weight, preferred_element_type=jnp.float32).astype(jnp.bfloat16)
    key_new = (
        jnp.dot(normed, key_weight, preferred_element_type=jnp.float32)
        .astype(jnp.bfloat16)
        .reshape(rows_here, key_heads, HD)
    )
    value_new = (
        jnp.dot(normed, value_weight, preferred_element_type=jnp.float32)
        .astype(jnp.bfloat16)
        .reshape(rows_here, key_heads, HD)
    )
    log_forget = jax.nn.log_sigmoid(
        jnp.dot(normed, forget_weight, preferred_element_type=jnp.float32) + forget_bias
    )
    positions = jnp.arange(cache_len, dtype=jnp.int32)
    is_last = positions[None, :] == (lengths - 1)[:, None]
    new_logsum = jnp.sum(jnp.where(is_last[:, None, :], cache_logsum, 0.0), axis=-1) + log_forget
    grouped = queries.reshape(rows_here, key_heads, group_size, HD)
    scores = jnp.einsum("sgjd,sgdp->sgjp", grouped, cache_keys, preferred_element_type=jnp.float32)
    scores = scores.reshape(rows_here, query_heads, cache_len) * score_scale
    scores = scores + new_logsum[:, :, None] - cache_logsum
    is_live = positions[None, :] < lengths[:, None]
    scores = jnp.where(is_live[:, None, :], scores, -jnp.inf)
    own_score = (
        jnp.einsum("sgjd,sgd->sgj", grouped, key_new, preferred_element_type=jnp.float32).reshape(
            rows_here, query_heads
        )
        * score_scale
    )
    top_score = jnp.maximum(jnp.max(scores, axis=-1), own_score)
    past_exp = jnp.exp(scores - top_score[:, :, None])
    own_exp = jnp.exp(own_score - top_score)
    denominator = jnp.sum(past_exp, axis=-1) + own_exp
    past_weight = (past_exp / denominator[:, :, None]).astype(jnp.bfloat16)
    own_weight = (own_exp / denominator).astype(jnp.bfloat16)
    attended = jnp.einsum(
        "sgjp,sgdp->sgjd",
        past_weight.reshape(rows_here, key_heads, group_size, cache_len),
        cache_values,
        preferred_element_type=jnp.float32,
    )
    attended = (
        attended
        + own_weight.astype(jnp.float32).reshape(rows_here, key_heads, group_size)[:, :, :, None]
        * value_new.astype(jnp.float32)[:, :, None, :]
    )
    attended = attended.reshape(rows_here, query_heads * HD).astype(jnp.bfloat16)
    whole_heads = lax.all_gather(attended, "tp", axis=1, tiled=True)
    projected = lax.dot_general(
        lax.all_gather(whole_heads, "ep", axis=0, tiled=True),
        out_weight,
        (((1,), (1,)), ((), ())),
        preferred_element_type=jnp.float32,
    ).astype(jnp.bfloat16)
    mixed = lax.all_to_all(projected, "ep", split_axis=0, concat_axis=1, tiled=True)
    residual = hidden.astype(jnp.float32) + mixed.astype(jnp.float32)
    ffn_in = root_norm(residual, ffn_gain).astype(jnp.bfloat16)
    ep_size = lax.axis_size("ep")
    local_experts = gate_weights.shape[0]
    experts = ep_size * local_experts
    route_count = rows_here * TOP_K
    capacity = 2 * ((route_count + experts - 1) // experts)
    flat_ids = expert_ids.reshape(route_count)
    onehot = (flat_ids[:, None] == jnp.arange(experts, dtype=jnp.int32)[None, :]).astype(jnp.int32)
    running = jnp.cumsum(onehot, axis=0)
    slot_index = jnp.sum(running * onehot, axis=1) - 1
    target = flat_ids * capacity + slot_index
    dispatch_map = (
        target[:, None] == jnp.arange(experts * capacity, dtype=jnp.int32)[None, :]
    ).astype(jnp.bfloat16)
    route_rows = jnp.repeat(ffn_in, TOP_K, axis=0)
    outgoing = lax.dot_general(
        dispatch_map, route_rows, (((0,), (0,)), ((), ())), preferred_element_type=jnp.float32
    )
    outgoing = outgoing.astype(jnp.bfloat16).reshape(
        ep_size, local_experts, capacity, ffn_in.shape[1]
    )
    arrived = lax.all_to_all(outgoing, "ep", split_axis=0, concat_axis=0, tiled=True)
    gate_act = jnp.einsum(
        "sekd,edf->sekf", arrived, gate_weights, preferred_element_type=jnp.float32
    )
    up_act = jnp.einsum("sekd,edf->sekf", arrived, up_weights, preferred_element_type=jnp.float32)
    hidden_act = (jax.nn.silu(gate_act) * up_act).astype(jnp.bfloat16)
    partial_out = jnp.einsum(
        "sekf,efd->sekd", hidden_act, down_weights, preferred_element_type=jnp.float32
    )
    half_sum = lax.psum_scatter(
        partial_out.astype(jnp.bfloat16), "tp", scatter_dimension=3, tiled=True
    )
    sent_back = lax.all_to_all(half_sum, "ep", split_axis=0, concat_axis=0, tiled=True)
    share_width = sent_back.shape[-1]
    picked = jnp.dot(
        dispatch_map,
        sent_back.reshape(experts * capacity, share_width),
        preferred_element_type=jnp.float32,
    )
    route_weight = expert_scores / jnp.sum(expert_scores, axis=-1, keepdims=True)
    expert_mix = jnp.sum(
        picked.reshape(rows_here, TOP_K, share_width) * route_weight[:, :, None], axis=1
    )
    own_part = lax.dynamic_slice_in_dim(
        residual, lax.axis_index("tp") * share_width, share_width, 1
    )
    updated = lax.all_gather((own_part + expert_mix).astype(jnp.bfloat16), "tp", axis=1, tiled=True)
    return (updated, key_new, value_new, new_logsum)


def solution(mesh):
    in_specs = (
        P("ep", None),
        P(),
        P(None, "tp"),
        P(None, "tp"),
        P(None, "tp"),
        P(None, "tp"),
        P("tp"),
        P("ep", "tp", None, None),
        P("ep", "tp", None, None),
        P("ep", "tp", None),
        P("ep"),
        P("ep", None),
        P(),
        P("ep", None),
        P("ep", None),
        P("ep", None, "tp"),
        P("ep", None, "tp"),
        P("ep", "tp", None),
    )
    out_specs = (P("ep", None), P("ep", "tp", None), P("ep", "tp", None), P("ep", "tp"))
    return jax.shard_map(
        per_device, mesh=mesh, in_specs=in_specs, out_specs=out_specs, check_vma=False
    )
```

profile of v0, /device:TPU:0, one launch (start us, length us, event | category | flops | bytes accessed | tf_op | source)
XLA Modules:
  0.0 167.7 jit_solution(6196648160617285266)
XLA Ops:
  7.2 0.8 broadcast_add_fusion.1
  8.0 0.7 iota_compare_fusion.4
  8.8 0.7 convert_element_type.86
  9.5 1.0 fusion.48
  10.5 3.0 %convolution_convert_fusion.3 = bf16[16,1024]{1,0:T(8,128)(2,1)S(1)} fusion(bf16[2048,1024]{1,0:T(8,128)(2,1)} %param.20, bf16[16,2048]{1,0:T(8,128)(2,1)} %param.18, f32[2048]{0:T(1024)S(1)} %convert_element_type.86, f32[16]{0:T(128)S(1)} %add_rsqrt_fusion.1), kind=kOutput, calls=%fused_computation.21 | convolution fusion | flops 67256320 | bytes 4300864 | tf_op jit(solution)/shard_map/dot_general | solution.py:44
  13.5 0.1 reshape.203
  13.6 0.1 iota_compare_fusion.3
  13.7 1.2 convolution_convert_fusion.5
  14.9 0.2 select_reduce_fusion
  15.1 0.1 fusion.59
  15.2 0.2 fusion.58
  15.5 0.5 fusion.68
  16.1 0.0 copy-done.8
  16.1 0.3 fusion.31
  16.5 0.8 fusion.69
  17.3 0.7 fusion.23
  18.0 0.1 convert_element_type.96
  18.2 2.1 %all_gather.9 = bf16[16,2048]{1,0:T(8,128)(2,1)} all-gather(bf16[16,1024]{1,0:T(8,128)(2,1)S(1)} %convert_element_type.96), channel_id=1, replica_groups=mesh['ep'=16,'tp'=2] {'tp'}, dimensions={1}, use_global_device_ids=true | all-gather | bytes 98304 | tf_op jit(solution)/shard_map/all_gather | solution.py:91
  20.3 0.1 copy.41
  20.4 0.1 eq.67
  20.5 0.1 fusion.56
  20.6 0.1 reduce_window_sum.11
  20.7 0.2 select_reduce_fusion.1
  20.9 57.2 %all-gather.2.cloned.1.call-done = bf16[256,2048]{1,0:T(8,128)(2,1)} async-done(((bf16[16,2048]{1,0:T(8,128)(2,1)}), bf16[256,2048]{1,0:T(8,128)(2,1)}) %all-gather.2.cloned.1.call-update) | async-done | bytes 1048592 | tf_op jit(solution)/shard_map/all_gather | solution.py:93
  78.1 2.3 %convolution_convert_fusion.2 = bf16[256,128]{1,0:T(8,128)(2,1)} fusion(bf16[256,2048]{1,0:T(8,128)(2,1)} %all-gather.2.cloned.1.call-done, bf16[128,2048]{1,0:T(8,128)(2,1)S(1)} %copy-done.4), kind=kOutput, calls=%fused_computation.20 | convolution fusion | flops 134250496 | bytes 1638400 | tf_op jit(solution)/shard_map/dot_general | solution.py:92
  80.4 4.5 %all-to-all-start = ((bf16[16,16,128]{2,1,0:T(8,128)(2,1)}), bf16[16,16,128]{2,1,0:T(8,128)(2,1)S(1)}, u32[]{:S(2)}, u32[]{:S(2)}) async-start(bf16[16,16,128]{2,1,0:T(8,128)(2,1)} %bitcast.5), calls=%async_computation | async-start | bytes 131072 | tf_op jit(solution)/shard_map/all_to_all | solution.py:98
  85.0 7.5 %all-to-all-done = bf16[16,16,128]{2,1,0:T(8,128)(2,1)S(1)} async-done(((bf16[16,16,128]{2,1,0:T(8,128)(2,1)}), bf16[16,16,128]{2,1,0:T(8,128)(2,1)S(1)}, u32[]{:S(2)}, u32[]{:S(2)}) %all-to-all-start) | async-done | bytes 65568 | tf_op jit(solution)/shard_map/all_to_all | solution.py:98
  92.4 0.1 multiply_reduce_fusion
  92.6 0.1 multiply_convert_fusion
  92.7 0.1 broadcast_in_dim.26
  92.7 0.1 reshape.206
  92.9 1.4 convolution_convert_fusion.1
  94.2 1.3 reshape.207
  95.5 25.9 %all_to_all.23 = bf16[16,1,12,2048]{3,2,1,0:T(8,128)(2,1)S(1)} all-to-all(bf16[16,1,12,2048]{3,2,1,0:T(8,128)(2,1)S(1)} %bitcast.98), channel_id=1, replica_groups=mesh['ep'=16,'tp'=2] {'ep'}, dimensions={0} | all-to-all | bytes 1572864 | tf_op jit(solution)/shard_map/all_to_all | solution.py:121
  121.4 1.0 copy-done.3
  122.4 0.6 convolution_bitcast_fusion.1
  123.0 0.6 copy-done.12
  123.6 3.5 %fusion = bf16[16,1,12,2048]{3,0,2,1:T(8,128)(2,1)} fusion(bf16[1,256,2048]{2,1,0:T(8,128)(2,1)S(1)} %copy-done.12, bf16[1,2048,256]{2,1,0:T(8,128)(2,1)} %param.34, bf16[16,1,12,2048]{3,2,1,0:T(8,128)(2,1)} %copy-done.3, f32[16,1,12,256]{3,0,2,1:T(8,128)S(1)} %convolution_bitcast_fusion.1), kind=kOutput, calls=%fused_computation.2 | convolution fusion | flops 403341312 | bytes 3866624 | tf_op jit(solution)/shard_map/sekf,efd->sekd/dot_general | solution.py:127
  127.2 6.6 %reduce-scatter.2.cloned.1.call-done = bf16[16,1,12,1024]{3,0,2,1:T(8,128)(2,1)} async-done(((bf16[16,1,12,2048]{3,0,2,1:T(8,128)(2,1)}), bf16[16,1,12,1024]{3,0,2,1:T(8,128)(2,1)}) %reduce-scatter.2.cloned.1.call-update) | async-done | bytes 393232 | tf_op jit(solution)/shard_map/reduce_scatter | solution.py:130
  133.7 2.0 %copy.45 = bf16[16,1,12,1024]{3,2,1,0:T(8,128)(2,1)} copy(bf16[16,1,12,1024]{3,0,2,1:T(8,128)(2,1)} %reduce-scatter.2.cloned.1.call-done) | data formatting | bytes 786432 | tf_op jit(solution)/shard_map/reduce_scatter | solution.py:130
  135.7 6.7 %all-to-all-start.2 = ((bf16[16,1,12,1024]{3,2,1,0:T(8,128)(2,1)}), bf16[16,1,12,1024]{3,2,1,0:T(8,128)(2,1)S(1)}, u32[]{:S(2)}, u32[]{:S(2)}) async-start(bf16[16,1,12,1024]{3,2,1,0:T(8,128)(2,1)} %copy.45), calls=%async_computation.3 | async-start | bytes 1048576 | tf_op jit(solution)/shard_map/all_to_all | solution.py:133
  142.5 0.1 sub.33
  142.5 0.1 copy.42
  142.7 15.3 %all-to-all-done.2 = bf16[16,1,12,1024]{3,2,1,0:T(8,128)(2,1)S(1)} async-done(((bf16[16,1,12,1024]{3,2,1,0:T(8,128)(2,1)}), bf16[16,1,12,1024]{3,2,1,0:T(8,128)(2,1)S(1)}, u32[]{:S(2)}, u32[]{:S(2)}) %all-to-all-start.2) | async-done | bytes 393248 | tf_op jit(solution)/shard_map/all_to_all | solution.py:133
  158.0 0.1 reshape.222
  158.0 0.3 fusion.17
  158.3 1.9 %all_gather.11 = bf16[16,2048]{1,0:T(8,128)(2,1)S(1)} all-gather(bf16[16,1024]{1,0:T(8,128)(2,1)S(1)} %add_convert_fusion), channel_id=1, replica_groups=mesh['ep'=16,'tp'=2] {'tp'}, dimensions={1}, use_global_device_ids=true | all-gather | bytes 98304 | tf_op jit(solution)/shard_map/all_gather | solution.py:147
  160.2 0.6 copy.63
  (43 shorter events, 0.3 us)
Async XLA Ops:
  7.2 8.3 %copy-start = (bf16[16,1,64,1024]{3,2,1,0:T(8,128)(2,1)S(1)}, bf16[16,1,64,1024]{3,2,1,0:T(8,128)(2,1)}, u32[]{:S(2)}) copy-start(bf16[16,1,64,1024]{3,2,1,0:T(8,128)(2,1)} %param.25) | copy-start | bytes 6291460
  7.2 71.0 %all-gather.2.cloned.1.call-start = ((), (), s32[]{:S(2)}) async-start(), calls=%async_computation.4 | async-start | bytes 1114112 | tf_op jit(solution)/shard_map/all_gather | solution.py:93
  10.4 3.3 %copy-start.2 = (bf16[16,2048]{1,0:T(8,128)(2,1)S(1)}, bf16[16,2048]{1,0:T(8,128)(2,1)}, u32[]{:S(2)}) copy-start(bf16[16,2048]{1,0:T(8,128)(2,1)} %param.18) | copy-start | bytes 196612
  10.4 4.4 %copy-start.1 = (f32[16,16,1024]{2,1,0:T(8,128)S(1)}, f32[16,16,1024]{2,1,0:T(8,128)}, u32[]{:S(2)}) copy-start(f32[16,16,1024]{2,1,0:T(8,128)} %param.27) | copy-start | bytes 3145732
  10.5 4.8 %copy-start.13 = (bf16[2048,16]{0,1:T(8,128)(2,1)S(1)}, bf16[2048,16]{0,1:T(8,128)(2,1)}, u32[]{:S(2)}) copy-start(bf16[2048,16]{0,1:T(8,128)(2,1)} %param.23) | copy-start | bytes 196612
  10.5 4.8 %copy-start.14 = (f32[16]{0:T(128)S(1)}, f32[16]{0:T(128)}, u32[]{:S(2)}) copy-start(f32[16]{0:T(128)} %param.24) | copy-start | bytes 196
  14.9 1.2 copy-start.15
  15.5 0.6 copy-start.8
  15.5 1.0 copy-start.5
  15.5 1.8 %copy-start.10 = (bf16[16,1,64,1024]{3,2,1,0:T(8,128)(2,1)S(1)}, bf16[16,1,64,1024]{3,2,1,0:T(8,128)(2,1)}, u32[]{:S(2)}) copy-start(bf16[16,1,64,1024]{3,2,1,0:T(8,128)(2,1)} %param.26) | copy-start | bytes 6291460
  17.3 3.0 %copy-start.9 = (bf16[2048]{0:T(1024)(128)(2,1)S(1)}, bf16[2048]{0:T(1024)(128)(2,1)}, u32[]{:S(2)}) copy-start(bf16[2048]{0:T(1024)(128)(2,1)} %param.30) | copy-start | bytes 12292
  17.3 3.0 %copy-start.6 = (s32[16,6]{0,1:T(8,128)S(1)}, s32[16,6]{0,1:T(8,128)}, u32[]{:S(2)}) copy-start(s32[16,6]{0,1:T(8,128)} %param.31) | copy-start | bytes 1156
  17.3 60.8 %copy-start.4 = (bf16[128,2048]{1,0:T(8,128)(2,1)S(1)}, bf16[128,2048]{1,0:T(8,128)(2,1)}, u32[]{:S(2)}) copy-start(bf16[128,2048]{1,0:T(8,128)(2,1)} %param.29) | copy-start | bytes 1572868
  80.4 12.0 %all-to-all-start = ((bf16[16,16,128]{2,1,0:T(8,128)(2,1)}), bf16[16,16,128]{2,1,0:T(8,128)(2,1)S(1)}, u32[]{:S(2)}, u32[]{:S(2)}) async-start(bf16[16,16,128]{2,1,0:T(8,128)(2,1)} %bitcast.5), calls=%async_computation | async-start | bytes 131072 | tf_op jit(solution)/shard_map/all_to_all | solution.py:98
  84.9 48.8 %reduce-scatter.2.cloned.1.call-start = ((), (), s32[]{:S(2)}) async-start(), calls=%async_computation.5 | async-start | bytes 1179648 | tf_op jit(solution)/shard_map/reduce_scatter | solution.py:130
  95.5 26.9 %copy-start.11 = (bf16[1,2048,256]{2,1,0:T(8,128)(2,1)S(1)}, bf16[1,2048,256]{2,1,0:T(8,128)(2,1)}, u32[]{:S(2)}) copy-start(bf16[1,2048,256]{2,1,0:T(8,128)(2,1)} %param.33) | copy-start | bytes 3145732
  121.4 1.0 copy-start.3
  122.4 1.2 copy-start.12
  127.1 15.5 %copy-start.7 = (f32[16,6]{0,1:T(8,128)S(1)}, f32[16,6]{0,1:T(8,128)}, u32[]{:S(2)}) copy-start(f32[16,6]{0,1:T(8,128)} %param.32) | copy-start | bytes 1156
  135.7 22.2 %all-to-all-start.2 = ((bf16[16,1,12,1024]{3,2,1,0:T(8,128)(2,1)}), bf16[16,1,12,1024]{3,2,1,0:T(8,128)(2,1)S(1)}, u32[]{:S(2)}, u32[]{:S(2)}) async-start(bf16[16,1,12,1024]{3,2,1,0:T(8,128)(2,1)} %copy.45), calls=%async_computation.3 | async-start | bytes 1048576 | tf_op jit(solution)/shard_map/all_to_all | solution.py:133
Sparse Core Ops, SparseCore 0:
  20.4 57.6 all-gather.1
  127.3 6.3 reduce-scatter.1
where the time goes:
time: 168 us
  waiting for transfers between devices  86.5 us (51%)
  blocking collectives  29.9 us (18%)
  matrix products  14.7 us (9%)
  between operations  14.3 us (9%)
  starting transfers between devices  11.3 us (7%)
  local copies, waits for them, and re-layouts  6.49 us (4%)
  other arithmetic  4.48 us (3%)
    all_gather x1, waiting for transfers between devices, per_device(): lax.all_gather(whole_heads, 'ep', axis=0, tiled=True)  57.2 us
    all_to_all x1, blocking collectives, per_device(): lax.all_to_all(outgoing, 'ep', split_axis=0, concat_axis=0, tiled=True)  25.9 us
    all_to_all x1, waiting for transfers between devices, per_device(): lax.all_to_all(half_sum, 'ep', split_axis=0, concat_axis=0, tiled=True)  15.3 us
    all_to_all x1, waiting for transfers between devices, per_device(): lax.all_to_all(projected, 'ep', split_axis=0, concat_axis=1, tiled=True)  7.47 us
    all_to_all x1, starting transfers between devices, per_device(): lax.all_to_all(half_sum, 'ep', split_axis=0, concat_axis=0, tiled=True)  6.74 us
    reduce_scatter x1, waiting for transfers between devices, per_device(): lax.psum_scatter(partial_out.astype(jnp.bfloat16), 'tp', scatter_dimensio...  6.55 us
    all_to_all x1, starting transfers between devices, per_device(): lax.all_to_all(projected, 'ep', split_axis=0, concat_axis=1, tiled=True)  4.46 us
    dot_general x1, matrix products, per_device(): jnp.einsum('sekf,efd->sekd', hidden_act, down_weights, preferred_element_...  3.53 us
  transfers between devices with their start and end apart: 4, of which 4 were waited for; matrix products, arithmetic and copies ran while one was open for 0% of the time, Pallas kernels for 0%

commit v1 on v0

--- a/solution.py
+++ b/solution.py
@@ -95,7 +95,10 @@
         (((1,), (1,)), ((), ())),
         preferred_element_type=jnp.float32,
     ).astype(jnp.bfloat16)
-    mixed = lax.all_to_all(projected, "ep", split_axis=0, concat_axis=1, tiled=True)
+    mixed = jnp.concatenate(
+        lax.all_to_all(jnp.stack(jnp.split(projected, lax.axis_size("ep"), 0), axis=0), "ep", 0, 0),
+        1,
+    )
     residual = hidden.astype(jnp.float32) + mixed.astype(jnp.float32)
     ffn_in = root_norm(residual, ffn_gain).astype(jnp.bfloat16)
     ep_size = lax.axis_size("ep")

time: 168 us -> 177 us (1.054)
  local copies, waits for them, and re-layouts: 6.49 us -> 16 us
    unnamed x34 -> x49, local copies, waits for them, and re-layouts: 2.45 us -> 11.3 us
where the time goes in v1:
time: 177 us
  waiting for transfers between devices  86.5 us (49%)
  blocking collectives  29.9 us (17%)
  local copies, waits for them, and re-layouts  16 us (9%)
  between operations  14.4 us (8%)
  matrix products  14 us (8%)
  starting transfers between devices  11.3 us (6%)
  other arithmetic  4.48 us (3%)
    all_gather x1, waiting for transfers between devices, per_device(): lax.all_gather(whole_heads, 'ep', axis=0, tiled=True)  57.2 us
    all_to_all x1, blocking collectives, per_device(): lax.all_to_all(outgoing, 'ep', split_axis=0, concat_axis=0, tiled=True)  25.9 us
    all_to_all x1, waiting for transfers between devices, per_device(): lax.all_to_all(half_sum, 'ep', split_axis=0, concat_axis=0, tiled=True)  15.3 us
    unnamed x49, local copies, waits for them, and re-layouts  11.3 us
    all_to_all x1, waiting for transfers between devices, per_device(): lax.all_to_all(jnp.stack(jnp.split(projected, lax.axis_size('ep'), 0), ax...  7.47 us
    all_to_all x1, starting transfers between devices, per_device(): lax.all_to_all(half_sum, 'ep', split_axis=0, concat_axis=0, tiled=True)  6.74 us
    reduce_scatter x1, waiting for transfers between devices, per_device(): lax.psum_scatter(partial_out.astype(jnp.bfloat16), 'tp', scatter_dimensio...  6.55 us
    all_to_all x1, starting transfers between devices, per_device(): lax.all_to_all(jnp.stack(jnp.split(projected, lax.axis_size('ep'), 0), ax...  4.46 us
  transfers between devices with their start and end apart: 4, of which 4 were waited for; matrix products, arithmetic and copies ran while one was open for 0% of the time, Pallas kernels for 0%

profile of v1, /device:TPU:0, one launch (start us, length us, event | category | flops | bytes accessed | tf_op | source)
XLA Modules:
  0.0 176.5 jit_solution(2353030339799074804)
XLA Ops:
  7.2 0.8 broadcast_add_fusion.1
  8.0 0.7 iota_compare_fusion.4
  8.8 0.7 convert_element_type.86
  9.5 1.0 fusion.48
  10.5 3.0 %convolution_convert_fusion.3 = bf16[16,1024]{1,0:T(8,128)(2,1)S(1)} fusion(bf16[2048,1024]{1,0:T(8,128)(2,1)} %param.20, bf16[16,2048]{1,0:T(8,128)(2,1)} %param.18, f32[2048]{0:T(1024)S(1)} %convert_element_type.86, f32[16]{0:T(128)S(1)} %add_rsqrt_fusion.1), kind=kOutput, calls=%fused_computation.21 | convolution fusion | flops 67256320 | bytes 4300864 | tf_op jit(solution)/shard_map/dot_general | solution.py:44
  13.7 1.2 convolution_convert_fusion.5
  14.9 0.2 select_reduce_fusion
  15.2 0.2 fusion.58
  15.5 0.5 fusion.68
  16.1 0.3 fusion.31
  16.5 0.8 fusion.69
  17.3 0.7 fusion.23
  18.2 2.1 %all_gather.9 = bf16[16,2048]{1,0:T(8,128)(2,1)} all-gather(bf16[16,1024]{1,0:T(8,128)(2,1)S(1)} %convert_element_type.96), channel_id=1, replica_groups=mesh['ep'=16,'tp'=2] {'tp'}, dimensions={1}, use_global_device_ids=true | all-gather | bytes 98304 | tf_op jit(solution)/shard_map/all_gather | solution.py:91
  20.7 0.2 select_reduce_fusion.1
  20.9 57.2 %all-gather.2.cloned.1.call-done = bf16[256,2048]{1,0:T(8,128)(2,1)} async-done(((bf16[16,2048]{1,0:T(8,128)(2,1)}), bf16[256,2048]{1,0:T(8,128)(2,1)}) %all-gather.2.cloned.1.call-update) | async-done | bytes 1048592 | tf_op jit(solution)/shard_map/all_gather | solution.py:93
  78.1 1.7 convolution_convert_fusion.2
  79.8 0.6 constant_dynamic-update-slice_fusion.15
  80.4 0.6 constant_dynamic-update-slice_fusion.14
  81.0 0.6 constant_dynamic-update-slice_fusion.13
  81.6 0.6 constant_dynamic-update-slice_fusion.12
  82.2 0.6 constant_dynamic-update-slice_fusion.11
  82.8 0.6 constant_dynamic-update-slice_fusion.10
  83.4 0.6 constant_dynamic-update-slice_fusion.9
  84.0 0.6 constant_dynamic-update-slice_fusion.8
  84.6 0.6 constant_dynamic-update-slice_fusion.7
  85.1 0.6 constant_dynamic-update-slice_fusion.6
  85.7 0.6 constant_dynamic-update-slice_fusion.5
  86.3 0.6 constant_dynamic-update-slice_fusion.4
  86.9 0.6 constant_dynamic-update-slice_fusion.3
  87.5 0.6 constant_dynamic-update-slice_fusion.2
  88.1 0.6 constant_dynamic-update-slice_fusion.1
  88.7 0.6 constant_dynamic-update-slice_fusion
  89.3 4.5 %all-to-all-start = ((bf16[16,16,128]{2,1,0:T(8,128)(2,1)}), bf16[16,16,128]{2,1,0:T(8,128)(2,1)S(1)}, u32[]{:S(2)}, u32[]{:S(2)}) async-start(bf16[16,16,128]{2,1,0:T(8,128)(2,1)} %constant_dynamic-update-slice_fusion), calls=%async_computation | async-start | bytes 131072 | tf_op jit(solution)/shard_map/all_to_all | solution.py:99
  93.8 7.5 %all-to-all-done = bf16[16,16,128]{2,1,0:T(8,128)(2,1)S(1)} async-done(((bf16[16,16,128]{2,1,0:T(8,128)(2,1)}), bf16[16,16,128]{2,1,0:T(8,128)(2,1)S(1)}, u32[]{:S(2)}, u32[]{:S(2)}) %all-to-all-start) | async-done | bytes 65568 | tf_op jit(solution)/shard_map/all_to_all | solution.py:99
  101.8 1.4 convolution_convert_fusion.1
  103.1 1.3 reshape.206
  104.4 25.9 %all_to_all.15 = bf16[16,1,12,2048]{3,2,1,0:T(8,128)(2,1)S(1)} all-to-all(bf16[16,1,12,2048]{3,2,1,0:T(8,128)(2,1)S(1)} %bitcast.161), channel_id=1, replica_groups=mesh['ep'=16,'tp'=2] {'ep'}, dimensions={0} | all-to-all | bytes 1572864 | tf_op jit(solution)/shard_map/all_to_all | solution.py:124
  130.3 1.0 copy-done.3
  131.3 0.6 convolution_bitcast_fusion.1
  131.9 0.6 copy-done.12
  132.5 3.5 %fusion = bf16[16,1,12,2048]{3,0,2,1:T(8,128)(2,1)} fusion(bf16[1,256,2048]{2,1,0:T(8,128)(2,1)S(1)} %copy-done.12, bf16[1,2048,256]{2,1,0:T(8,128)(2,1)} %param.34, bf16[16,1,12,2048]{3,2,1,0:T(8,128)(2,1)} %copy-done.3, f32[16,1,12,256]{3,0,2,1:T(8,128)S(1)} %convolution_bitcast_fusion.1), kind=kOutput, calls=%fused_computation.2 | convolution fusion | flops 403341312 | bytes 3866624 | tf_op jit(solution)/shard_map/sekf,efd->sekd/dot_general | solution.py:130
  136.0 6.6 %reduce-scatter.2.cloned.1.call-done = bf16[16,1,12,1024]{3,0,2,1:T(8,128)(2,1)} async-done(((bf16[16,1,12,2048]{3,0,2,1:T(8,128)(2,1)}), bf16[16,1,12,1024]{3,0,2,1:T(8,128)(2,1)}) %reduce-scatter.2.cloned.1.call-update) | async-done | bytes 393232 | tf_op jit(solution)/shard_map/reduce_scatter | solution.py:133
  142.6 2.0 %copy.44 = bf16[16,1,12,1024]{3,2,1,0:T(8,128)(2,1)} copy(bf16[16,1,12,1024]{3,0,2,1:T(8,128)(2,1)} %reduce-scatter.2.cloned.1.call-done) | data formatting | bytes 786432 | tf_op jit(solution)/shard_map/reduce_scatter | solution.py:133
  144.6 6.7 %all-to-all-start.2 = ((bf16[16,1,12,1024]{3,2,1,0:T(8,128)(2,1)}), bf16[16,1,12,1024]{3,2,1,0:T(8,128)(2,1)S(1)}, u32[]{:S(2)}, u32[]{:S(2)}) async-start(bf16[16,1,12,1024]{3,2,1,0:T(8,128)(2,1)} %copy.44), calls=%async_computation.3 | async-start | bytes 1048576 | tf_op jit(solution)/shard_map/all_to_all | solution.py:136
  151.6 15.3 %all-to-all-done.2 = bf16[16,1,12,1024]{3,2,1,0:T(8,128)(2,1)S(1)} async-done(((bf16[16,1,12,1024]{3,2,1,0:T(8,128)(2,1)}), bf16[16,1,12,1024]{3,2,1,0:T(8,128)(2,1)S(1)}, u32[]{:S(2)}, u32[]{:S(2)}) %all-to-all-start.2) | async-done | bytes 393248 | tf_op jit(solution)/shard_map/all_to_all | solution.py:136
  166.9 0.3 fusion.17
  167.2 1.9 %all_gather.11 = bf16[16,2048]{1,0:T(8,128)(2,1)S(1)} all-gather(bf16[16,1024]{1,0:T(8,128)(2,1)S(1)} %add_convert_fusion), channel_id=1, replica_groups=mesh['ep'=16,'tp'=2] {'tp'}, dimensions={1}, use_global_device_ids=true | all-gather | bytes 98304 | tf_op jit(solution)/shard_map/all_gather | solution.py:150
  169.1 0.6 copy.77
  (59 shorter events, 1.9 us)
Async XLA Ops:
  7.2 8.3 %copy-start = (bf16[16,1,64,1024]{3,2,1,0:T(8,128)(2,1)S(1)}, bf16[16,1,64,1024]{3,2,1,0:T(8,128)(2,1)}, u32[]{:S(2)}) copy-start(bf16[16,1,64,1024]{3,2,1,0:T(8,128)(2,1)} %param.25) | copy-start | bytes 6291460
  7.2 71.0 %all-gather.2.cloned.1.call-start = ((), (), s32[]{:S(2)}) async-start(), calls=%async_computation.4 | async-start | bytes 1114112 | tf_op jit(solution)/shard_map/all_gather | solution.py:93
  10.4 3.3 %copy-start.2 = (bf16[16,2048]{1,0:T(8,128)(2,1)S(1)}, bf16[16,2048]{1,0:T(8,128)(2,1)}, u32[]{:S(2)}) copy-start(bf16[16,2048]{1,0:T(8,128)(2,1)} %param.18) | copy-start | bytes 196612
  10.4 4.4 %copy-start.1 = (f32[16,16,1024]{2,1,0:T(8,128)S(1)}, f32[16,16,1024]{2,1,0:T(8,128)}, u32[]{:S(2)}) copy-start(f32[16,16,1024]{2,1,0:T(8,128)} %param.27) | copy-start | bytes 3145732
  10.5 4.8 %copy-start.13 = (bf16[2048,16]{0,1:T(8,128)(2,1)S(1)}, bf16[2048,16]{0,1:T(8,128)(2,1)}, u32[]{:S(2)}) copy-start(bf16[2048,16]{0,1:T(8,128)(2,1)} %param.23) | copy-start | bytes 196612
  10.5 4.8 %copy-start.14 = (f32[16]{0:T(128)S(1)}, f32[16]{0:T(128)}, u32[]{:S(2)}) copy-start(f32[16]{0:T(128)} %param.24) | copy-start | bytes 196
  14.9 1.2 copy-start.15
  15.5 0.6 copy-start.8
  15.5 1.0 copy-start.5
  15.5 1.8 %copy-start.10 = (bf16[16,1,64,1024]{3,2,1,0:T(8,128)(2,1)S(1)}, bf16[16,1,64,1024]{3,2,1,0:T(8,128)(2,1)}, u32[]{:S(2)}) copy-start(bf16[16,1,64,1024]{3,2,1,0:T(8,128)(2,1)} %param.26) | copy-start | bytes 6291460
  17.3 3.0 %copy-start.9 = (bf16[2048]{0:T(1024)(128)(2,1)S(1)}, bf16[2048]{0:T(1024)(128)(2,1)}, u32[]{:S(2)}) copy-start(bf16[2048]{0:T(1024)(128)(2,1)} %param.30) | copy-start | bytes 12292
  17.3 3.0 %copy-start.6 = (s32[16,6]{0,1:T(8,128)S(1)}, s32[16,6]{0,1:T(8,128)}, u32[]{:S(2)}) copy-start(s32[16,6]{0,1:T(8,128)} %param.31) | copy-start | bytes 1156
  17.3 60.8 %copy-start.4 = (bf16[128,2048]{1,0:T(8,128)(2,1)S(1)}, bf16[128,2048]{1,0:T(8,128)(2,1)}, u32[]{:S(2)}) copy-start(bf16[128,2048]{1,0:T(8,128)(2,1)} %param.29) | copy-start | bytes 1572868
  89.3 12.0 %all-to-all-start = ((bf16[16,16,128]{2,1,0:T(8,128)(2,1)}), bf16[16,16,128]{2,1,0:T(8,128)(2,1)S(1)}, u32[]{:S(2)}, u32[]{:S(2)}) async-start(bf16[16,16,128]{2,1,0:T(8,128)(2,1)} %constant_dynamic-update-slice_fusion), calls=%async_computation | async-start | bytes 131072 | tf_op jit(solution)/shard_map/all_to_all | solution.py:99
  93.8 48.8 %reduce-scatter.2.cloned.1.call-start = ((), (), s32[]{:S(2)}) async-start(), calls=%async_computation.5 | async-start | bytes 1179648 | tf_op jit(solution)/shard_map/reduce_scatter | solution.py:133
  104.4 26.9 %copy-start.11 = (bf16[1,2048,256]{2,1,0:T(8,128)(2,1)S(1)}, bf16[1,2048,256]{2,1,0:T(8,128)(2,1)}, u32[]{:S(2)}) copy-start(bf16[1,2048,256]{2,1,0:T(8,128)(2,1)} %param.33) | copy-start | bytes 3145732
  130.3 1.0 copy-start.3
  131.2 1.2 copy-start.12
  136.0 15.5 %copy-start.7 = (f32[16,6]{0,1:T(8,128)S(1)}, f32[16,6]{0,1:T(8,128)}, u32[]{:S(2)}) copy-start(f32[16,6]{0,1:T(8,128)} %param.32) | copy-start | bytes 1156
  144.6 22.2 %all-to-all-start.2 = ((bf16[16,1,12,1024]{3,2,1,0:T(8,128)(2,1)}), bf16[16,1,12,1024]{3,2,1,0:T(8,128)(2,1)S(1)}, u32[]{:S(2)}, u32[]{:S(2)}) async-start(bf16[16,1,12,1024]{3,2,1,0:T(8,128)(2,1)} %copy.44), calls=%async_computation.3 | async-start | bytes 1048576 | tf_op jit(solution)/shard_map/all_to_all | solution.py:136
Sparse Core Ops, SparseCore 0:
  20.4 57.6 all-gather.1
  136.2 6.3 reduce-scatter.1
